TPU v7x, 128 devices: a whole 4x4x4 slice. The times are simulated.
128 devices in a mesh: fs: 16 (over z, y), tp: 8 (over x, core).
Axes of the slice: x: 4, y: 4, z: 4, core: 2. Of those that a mesh axis runs over, the one named last changes fastest.
Arguments:
- late_input: bfloat16 [8192, 2048], P(('fs', 'tp')), may hold values from -6 to 6
- early_input: bfloat16 [8192, 2048], P(('fs', 'tp')), may hold values from -6 to 6
- early_grad: bfloat16 [8192, 2048], P(('fs', 'tp')), may hold values from -24 to 24
- pre_gain: float32 [2048], replicated, may hold values from 0.1 to 1.9
- post_gain: float32 [2048], replicated, may hold values from 0.1 to 1.9
- gate_weight: bfloat16 [2048, 4096], P('fs', 'tp'), may hold values from -0.125 to 0.125
- up_weight: bfloat16 [2048, 4096], P('fs', 'tp'), may hold values from -0.125 to 0.125
- down_weight: bfloat16 [2048, 4096], P('fs', 'tp'), may hold values from -0.09375 to 0.09375
- gate_sum: float32 [2048, 4096], P('fs', 'tp'), may hold values from -1.8 to 1.8
- up_sum: float32 [2048, 4096], P('fs', 'tp'), may hold values from -1.8 to 1.8
- down_gradient_sum: float32 [2048, 4096], P('fs', 'tp'), may hold values from -1.8 to 1.8
Outputs:
- late_output: bfloat16 [8192, 2048], P(('fs', 'tp'))
- early_input_grad: bfloat16 [8192, 2048], P(('fs', 'tp'))
- gate_total: float32 [2048, 4096], P('fs', 'tp')
- up_total: float32 [2048, 4096], P('fs', 'tp')
- down_total: float32 [2048, 4096], P('fs', 'tp')
All inputs are finite; a program needn't handle non-finite values.
Results may differ from a plain program's by a relative error of at most 0.013.
Values may be sent and summed in bfloat16 or wider, within the bound.
A program may use at most 128 MiB of HBM per device.

v0:
```python
import math
import jax
import jax.numpy as jnp
from jax import lax
from jax.sharding import PartitionSpec as P

NORM_EPS = 1e-06


def sent_together(arrays, axis, dim, along):
    ends, at = ([], 0)
    for a in arrays[:-1]:
        at += a.shape[along]
        ends.append(at)
    both = jnp.concatenate(arrays, axis=along)
    return tuple(jnp.split(lax.all_gather(both, axis, axis=dim, tiled=True), ends, axis=along))


def sent_to_all(shard, axis):
    peers = lax.axis_size(axis)
    return lax.all_to_all(
        jnp.broadcast_to(shard[None], (peers, *shard.shape)), axis, 0, 0, tiled=True
    )


def in_order(parts, dim):
    parts = jnp.moveaxis(parts, 0, dim)
    dims = parts.shape
    return parts.reshape(*dims[:dim], dims[dim] * dims[dim + 1], *dims[dim + 2 :])


def gather_directly(shard, axis, dim):
    parts = sent_to_all(shard, axis)
    return in_order(parts, dim)


def in_blocks(shard, dim, peers):
    dims = shard.shape
    parts = shard.reshape(*dims[:dim], peers, dims[dim] // peers, *dims[dim + 1 :])
    return jnp.moveaxis(parts, dim, 0)


def summed_on_arrival(shard, axis, dim):
    parts = in_blocks(shard, dim, lax.axis_size(axis))
    arrived = lax.all_to_all(parts, axis, split_axis=0, concat_axis=0, tiled=True)
    return arrived.astype(jnp.float32).sum(axis=0)


def contract_last(first_op, second_op):
    return lax.dot_general(
        first_op, second_op, (((1,), (1,)), ((), ())), preferred_element_type=jnp.float32
    )


def contract_first(first_op, second_op):
    return lax.dot_general(
        first_op, second_op, (((0,), (0,)), ((), ())), preferred_element_type=jnp.float32
    )


def inverse_rms(values):
    return lax.rsqrt(jnp.mean(values * values, axis=-1, keepdims=True) + NORM_EPS)


def per_device(
    late_input,
    early_input,
    early_grad,
    pre_gain,
    post_gain,
    gate_weight,
    up_weight,
    down_weight,
    gate_sum,
    up_sum,
    down_gradient_sum,
):
    tok_rows, model_width = late_input.shape
    group_rows = tok_rows * lax.axis_size("tp")
    grad_scale = 1.0 / math.sqrt(group_rows * lax.axis_size("fs"))
    hidden_width = gate_sum.shape[1]
    input_rows = jnp.stack([late_input, early_input]).astype(jnp.float32)
    input_inverse = inverse_rms(input_rows)
    normed = (input_rows * input_inverse * pre_gain).astype(jnp.bfloat16)
    normed_rows = lax.all_gather(normed, "tp", axis=1, tiled=True)
    gate_all, up_all, down_gradient_rows = sent_together(
        (gate_weight, up_weight, down_weight), "fs", 0, 1
    )
    flat_rows = normed_rows.reshape(2 * group_rows, model_width)
    gate_pre = jnp.dot(flat_rows, gate_all, preferred_element_type=jnp.float32)
    up_pre = jnp.dot(flat_rows, up_all, preferred_element_type=jnp.float32)
    hidden_state = (
        (jax.nn.silu(gate_pre) * up_pre).astype(jnp.bfloat16).reshape(2, group_rows, hidden_width)
    )
    gated_product = jnp.einsum(
        "utx,ix->tui", hidden_state, down_gradient_rows, preferred_element_type=jnp.float32
    )
    mixed_sum = lax.psum_scatter(
        gated_product.reshape(lax.axis_size("tp") * tok_rows, 2 * model_width).astype(jnp.bfloat16),
        "tp",
        scatter_dimension=0,
        tiled=True,
    ).astype(jnp.float32)
    mixed_sum = lax.optimization_barrier(mixed_sum.astype(jnp.bfloat16)).astype(jnp.float32)
    mixed_sum = mixed_sum.reshape(tok_rows, 2, model_width)
    mixed_inverse = inverse_rms(mixed_sum)
    late_output = (input_rows[0] + 0.5 * mixed_sum[:, 0] * mixed_inverse[:, 0] * post_gain).astype(
        jnp.bfloat16
    )
    early_mixed = mixed_sum[:, 1]
    early_inverse_norm = mixed_inverse[:, 1]
    weighted = 0.5 * early_grad.astype(jnp.float32) * post_gain
    mixed_cot = (
        early_inverse_norm * weighted
        - early_mixed
        * early_inverse_norm**3
        * jnp.mean(weighted * early_mixed, axis=-1, keepdims=True)
    ).astype(jnp.bfloat16)
    cot_rows = gather_directly(mixed_cot, "tp", 0)
    early_hidden = hidden_state[1]
    early_normed = normed_rows[1]
    hidden_cot = jnp.dot(cot_rows, down_gradient_rows, preferred_element_type=jnp.float32)
    early_gate = gate_pre[group_rows:]
    early_up = up_pre[group_rows:]
    sigmoid_gate = jax.nn.sigmoid(early_gate)
    gate_cot = (
        hidden_cot * early_up * sigmoid_gate * (1.0 + early_gate * (1.0 - sigmoid_gate))
    ).astype(jnp.bfloat16)
    up_cot = (hidden_cot * early_gate * sigmoid_gate).astype(jnp.bfloat16)
    normed_cot = summed_on_arrival(
        (contract_last(gate_cot, gate_all) + contract_last(up_cot, up_all)).astype(jnp.bfloat16),
        "tp",
        0,
    )
    normed_cot = lax.optimization_barrier(normed_cot.astype(jnp.bfloat16)).astype(jnp.float32)
    weighted_in = normed_cot * pre_gain
    early_values = input_rows[1]
    early_in_inverse = input_inverse[1]
    early_input_grad = (
        early_grad.astype(jnp.float32)
        + early_in_inverse * weighted_in
        - early_values
        * early_in_inverse**3
        * jnp.mean(weighted_in * early_values, axis=-1, keepdims=True)
    ).astype(jnp.bfloat16)
    totals = lax.psum_scatter(
        (
            grad_scale
            * jnp.concatenate(
                [
                    contract_first(early_normed, gate_cot),
                    contract_first(early_normed, up_cot),
                    contract_first(cot_rows, early_hidden),
                ],
                1,
            )
        ).astype(jnp.bfloat16),
        "fs",
        scatter_dimension=0,
        tiled=True,
    ).astype(jnp.float32)
    gate_total = gate_sum + totals[:, :hidden_width]
    up_total = up_sum + totals[:, hidden_width : 2 * hidden_width]
    down_total = down_gradient_sum + totals[:, 2 * hidden_width :]
    return (late_output, early_input_grad, gate_total, up_total, down_total)


def solution(mesh):
    in_specs = (
        P(("fs", "tp"), None),
        P(("fs", "tp"), None),
        P(("fs", "tp"), None),
        P(),
        P(),
        P("fs", "tp"),
        P("fs", "tp"),
        P("fs", "tp"),
        P("fs", "tp"),
        P("fs", "tp"),
        P("fs", "tp"),
    )
    out_specs = (
        P(("fs", "tp"), None),
        P(("fs", "tp"), None),
        P("fs", "tp"),
        P("fs", "tp"),
        P("fs", "tp"),
    )
    return jax.shard_map(
        per_device, mesh=mesh, in_specs=in_specs, out_specs=out_specs, check_vma=False
    )
```

profile of v0, /device:TPU:0, one launch (start us, length us, event | category | flops | bytes accessed | tf_op | source)
XLA Modules:
  0.0 314.3 jit_solution(15130578604359886631)
XLA Ops:
  7.2 0.0 all-gather.5.cloned.1.call-start
  7.2 1.2 multiply_reduce_fusion.1
  8.4 2.0 multiply_convert_fusion.2
  10.5 0.0 all-gather.5.cloned.1.call-update
  10.5 0.0 all-gather.3.cloned.1.call-start
  10.5 1.8 pad_maximum_fusion
  12.4 0.0 all-gather.3.cloned.1.call-update
  12.4 0.0 reduce-scatter.5.cloned.1.call-start
  12.4 32.7 %all-gather.5.cloned.1.call-done = bf16[2,512,2048]{2,1,0:T(8,128)(2,1)} async-done(((bf16[2,64,2048]{2,1,0:T(8,128)(2,1)}), bf16[2,512,2048]{2,1,0:T(8,128)(2,1)}) %all-gather.5.cloned.1.call-update) | async-done | bytes 4194320 | tf_op jit(solution)/shard_map/all_gather | solution.py:85
  45.2 63.5 %all-gather.3.cloned.1.call-done = bf16[2048,1536]{1,0:T(8,128)(2,1)} async-done(((bf16[128,1536]{1,0:T(8,128)(2,1)}), bf16[2048,1536]{1,0:T(8,128)(2,1)}) %all-gather.3.cloned.1.call-update) | async-done | bytes 6291472 | tf_op jit(solution)/shard_map/all_gather | solution.py:16
  108.7 5.3 %fusion.9 = f32[1024,512]{1,0:T(8,128)S(1)} fusion(bf16[1024,2048]{1,0:T(8,128)(2,1)} %bitcast.66, bf16[2048,1536]{1,0:T(8,128)(2,1)} %all-gather.3.cloned.1.call-done), kind=kOutput, calls=%fused_computation.14 | convolution fusion | flops 2147483648 | bytes 8388608 | tf_op jit(solution)/shard_map/dot_general | solution.py:90
  114.0 0.0 copy-done
  114.0 0.6 copy-done.2
  114.6 3.9 %multiply_convert_fusion = (bf16[1024,512]{1,0:T(8,128)(2,1)S(1)}, f32[1024,512]{1,0:T(8,128)}) fusion(f32[1024,512]{1,0:T(8,128)S(1)} %fusion.9, bf16[1024,2048]{1,0:T(8,128)(2,1)S(1)} %bitcast.67, bf16[2048,1536]{1,0:T(8,128)(2,1)S(1)} %copy-done.2), kind=kOutput, calls=%fused_computation.6 | convolution fusion | flops 2150629376 | bytes 11534336 | tf_op jit(solution)/shard_map/dot_general | solution.py:91
  118.5 0.0 copy-done.12
  118.5 4.4 %convolution_convert_fusion = bf16[2048,2,512]{2,0,1:T(8,128)(2,1)} fusion(bf16[2,512,512]{2,1,0:T(8,128)(2,1)S(1)} %bitcast.75, bf16[2048,1536]{1,0:T(8,128)(2,1)S(1)} %copy-done.2), kind=kOutput, calls=%fused_computation.3 | convolution fusion | flops 2149580800 | bytes 7340032 | tf_op jit(solution)/shard_map/utx,ix->tui/dot_general | solution.py:95
  122.9 6.3 %copy.39 = bf16[512,4096]{1,0:T(8,128)(2,1)} copy(bf16[512,4096]{0,1:T(8,128)(2,1)} %bitcast.68) | data formatting | bytes 8388608 | tf_op jit(solution)/shard_map/convert_element_type | solution.py:99
  129.2 0.0 reduce-scatter.5.cloned.1.call-update
  129.3 0.0 reduce-scatter.7.cloned.1.call-start
  129.3 0.6 copy-done.11
  129.9 36.9 %reduce-scatter.5.cloned.1.call-done = bf16[64,4096]{1,0:T(8,128)(2,1)} async-done(((bf16[512,4096]{1,0:T(8,128)(2,1)}), bf16[64,4096]{1,0:T(8,128)(2,1)}) %reduce-scatter.5.cloned.1.call-update) | async-done | bytes 524304 | tf_op jit(solution)/shard_map/reduce_scatter | solution.py:98
  166.9 2.1 reshape.128
  168.9 1.6 fusion.31
  170.6 0.5 multiply_reduce_fusion
  171.1 0.1 copy.52
  171.1 0.0 copy-done.3
  171.1 0.3 fusion.21
  171.4 0.3 fusion.20
  171.7 0.2 broadcast_in_dim.2
  172.0 29.7 %all_to_all.10 = bf16[8,64,2048]{2,1,0:T(8,128)(2,1)S(1)} all-to-all(bf16[8,64,2048]{2,1,0:T(8,128)(2,1)S(1)} %broadcast_in_dim.2), channel_id=1, replica_groups=mesh['fs'=16,'tp'=8] {'tp'}, dimensions={0} | all-to-all | bytes 4194304 | tf_op jit(solution)/shard_map/all_to_all | solution.py:21
  201.6 1.3 fusion.24
  202.9 0.3 copy-done.13
  203.2 0.6 copy-done.14
  203.8 3.3 %multiply_convert_fusion.1 = (bf16[512,512]{1,0:T(8,128)(2,1)S(1)}, bf16[512,512]{1,0:T(8,128)(2,1)S(1)}) fusion(f32[1024,512]{1,0:T(8,128)S(1)} %copy-done.13, f32[1024,512]{1,0:T(8,128)S(1)} %copy-done.14, bf16[512,2048]{1,0:T(8,128)(2,1)S(1)} %bitcast.65, bf16[2048,1536]{1,0:T(8,128)(2,1)} %all-gather.3.cloned.1.call-done), kind=kOutput, calls=%fused_computation.23 | convolution fusion | flops 1077149696 | bytes 7340032 | tf_op jit(solution)/shard_map/dot_general | solution.py:122
  207.1 0.0 copy-done.1
  207.1 1.3 fusion.2
  208.4 1.3 fusion.3
  209.8 3.8 %fusion = bf16[2048,1536]{0,1:T(8,128)(2,1)} fusion(f32[2048,512]{0,1:T(8,128)S(1)} %fusion.24, f32[2048,512]{0,1:T(8,128)S(1)} %fusion.2, f32[2048,512]{0,1:T(8,128)S(1)} %fusion.3), kind=kLoop, calls=%fused_computation.1 | loop fusion | flops 12582912 | bytes 18874368 | tf_op jit(solution)/shard_map/convert_element_type | solution.py:157
  213.6 8.6 %copy.48 = bf16[2048,1536]{1,0:T(8,128)(2,1)} copy(bf16[2048,1536]{0,1:T(8,128)(2,1)} %fusion) | data formatting | bytes 12582912
  222.2 0.0 reduce-scatter.7.cloned.1.call-update
  222.3 2.9 fusion.7
  225.1 4.2 %add_convert_fusion = bf16[512,2048]{1,0:T(8,128)(2,1)} fusion(f32[512,2048]{1,0:T(8,128)S(1)} %fusion.7, bf16[512,512]{1,0:T(8,128)(2,1)S(1)} %get-tuple-element.25, bf16[2048,1536]{1,0:T(8,128)(2,1)} %all-gather.3.cloned.1.call-done), kind=kOutput, calls=%fused_computation.2 | convolution fusion | flops 1075838976 | bytes 8912896 | tf_op jit(solution)/shard_map/dot_general | solution.py:50
  229.4 3.8 %all-to-all-start.1 = ((bf16[8,64,2048]{2,1,0:T(8,128)(2,1)}), bf16[8,64,2048]{2,1,0:T(8,128)(2,1)S(1)}, u32[]{:S(2)}, u32[]{:S(2)}) async-start(bf16[8,64,2048]{2,1,0:T(8,128)(2,1)} %bitcast.14), calls=%async_computation.2 | async-start | bytes 4194304 | tf_op jit(solution)/shard_map/all_to_all | solution.py:45
  233.1 0.0 copy-done.7
  233.1 0.8 copy.44
  234.0 0.0 copy-done.8
  234.0 0.8 copy.43
  234.8 0.0 copy-done.9
  234.8 0.8 copy.42
  235.7 1.1 maximum_convert_fusion
  236.8 23.5 %all-to-all-done.1 = bf16[8,64,2048]{2,1,0:T(8,128)(2,1)S(1)} async-done(((bf16[8,64,2048]{2,1,0:T(8,128)(2,1)}), bf16[8,64,2048]{2,1,0:T(8,128)(2,1)S(1)}, u32[]{:S(2)}, u32[]{:S(2)}) %all-to-all-start.1) | async-done | bytes 2097184 | tf_op jit(solution)/shard_map/all_to_all | solution.py:45
  260.2 1.1 reduce_sum.51
  261.3 1.2 multiply_reduce_fusion.2
  262.6 2.2 fusion.23
  264.8 39.1 %reduce-scatter.7.cloned.1.call-done = bf16[128,1536]{1,0:T(8,128)(2,1)} async-done(((bf16[2048,1536]{1,0:T(8,128)(2,1)}), bf16[128,1536]{1,0:T(8,128)(2,1)}) %reduce-scatter.7.cloned.1.call-update) | async-done | bytes 393232
  303.8 1.2 copy.49
  305.1 0.1 convert_element_type.69
  305.1 0.0 copy-done.4
  305.1 0.0 copy-done.5
  305.1 0.0 copy-done.6
  305.2 0.1 slice_add_fusion
  305.2 0.8 copy.45
  306.1 0.8 copy.46
  306.9 0.8 copy.47
  (24 shorter events, 0.1 us)
Async XLA Ops:
  7.2 38.0 %all-gather.5.cloned.1.call-start = ((), (), s32[]{:S(2)}) async-start(), calls=%async_computation.5 | async-start | bytes 4718592 | tf_op jit(solution)/shard_map/all_gather | solution.py:85
  10.5 98.2 %all-gather.3.cloned.1.call-start = ((), (), s32[]{:S(2)}) async-start(), calls=%async_computation.4 | async-start | bytes 6684672 | tf_op jit(solution)/shard_map/all_gather | solution.py:16
  12.4 154.5 %reduce-scatter.5.cloned.1.call-start = ((), (), s32[]{:S(2)}) async-start(), calls=%async_computation.6 | async-start | bytes 4718592 | tf_op jit(solution)/shard_map/reduce_scatter | solution.py:98
  108.7 5.3 %copy-start = (bf16[2,512,2048]{2,1,0:T(8,128)(2,1)S(1)}, bf16[2,512,2048]{2,1,0:T(8,128)(2,1)}, u32[]{:S(2)}) copy-start(bf16[2,512,2048]{2,1,0:T(8,128)(2,1)} %all-gather.5.cloned.1.call-done) | copy-start | bytes 12582916
  108.7 5.9 %copy-start.2 = (bf16[2048,1536]{1,0:T(8,128)(2,1)S(1)}, bf16[2048,1536]{1,0:T(8,128)(2,1)}, u32[]{:S(2)}) copy-start(bf16[2048,1536]{1,0:T(8,128)(2,1)} %all-gather.3.cloned.1.call-done) | copy-start | bytes 18874372
  114.6 3.9 %copy-start.12 = (f32[1024,512]{1,0:T(8,128)}, f32[1024,512]{1,0:T(8,128)S(1)}, u32[]{:S(2)}) copy-start(f32[1024,512]{1,0:T(8,128)S(1)} %fusion.9) | copy-start | bytes 6291460
  129.2 0.7 copy-start.11
  129.2 41.9 %copy-start.3 = (bf16[64,2048]{1,0:T(8,128)(2,1)S(1)}, bf16[64,2048]{1,0:T(8,128)(2,1)}, u32[]{:S(2)}) copy-start(bf16[64,2048]{1,0:T(8,128)(2,1)} %param.13) | copy-start | bytes 786436
  129.3 174.6 %reduce-scatter.7.cloned.1.call-start = ((), (), s32[]{:S(2)}) async-start(), calls=%async_computation.7 | async-start | bytes 6684672
  201.6 1.6 copy-start.13
  201.6 2.2 copy-start.14
  203.8 3.3 %copy-start.1 = (bf16[2,512,2048]{2,1,0:T(8,128)(2,1)S(1)}, bf16[2,512,2048]{2,1,0:T(8,128)(2,1)}, u32[]{:S(2)}) copy-start(bf16[2,512,2048]{2,1,0:T(8,128)(2,1)} %all-gather.5.cloned.1.call-done) | copy-start | bytes 12582916
  229.4 3.8 %copy-start.7 = (f32[128,512]{1,0:T(8,128)S(1)}, f32[128,512]{1,0:T(8,128)}, u32[]{:S(2)}) copy-start(f32[128,512]{1,0:T(8,128)} %param.21) | copy-start | bytes 786436
  229.4 4.6 %copy-start.8 = (f32[128,512]{1,0:T(8,128)S(1)}, f32[128,512]{1,0:T(8,128)}, u32[]{:S(2)}) copy-start(f32[128,512]{1,0:T(8,128)} %param.20) | copy-start | bytes 786436
  229.4 5.5 %copy-start.9 = (f32[128,512]{1,0:T(8,128)S(1)}, f32[128,512]{1,0:T(8,128)}, u32[]{:S(2)}) copy-start(f32[128,512]{1,0:T(8,128)} %param.19) | copy-start | bytes 786436
  229.4 32.0 %copy-start.10 = (f32[2048]{0:T(1024)S(1)}, f32[2048]{0:T(1024)}, u32[]{:S(2)}) copy-start(f32[2048]{0:T(1024)} %param.14) | copy-start | bytes 24580
  229.4 30.9 %all-to-all-start.1 = ((bf16[8,64,2048]{2,1,0:T(8,128)(2,1)}), bf16[8,64,2048]{2,1,0:T(8,128)(2,1)S(1)}, u32[]{:S(2)}, u32[]{:S(2)}) async-start(bf16[8,64,2048]{2,1,0:T(8,128)(2,1)} %bitcast.14), calls=%async_computation.2 | async-start | bytes 4194304 | tf_op jit(solution)/shard_map/all_to_all | solution.py:45
  261.3 43.8 %copy-start.4 = (f32[128,512]{0,1:T(8,128)S(1)}, f32[128,512]{0,1:T(8,128)}, u32[]{:S(2)}) copy-start(f32[128,512]{0,1:T(8,128)} %copy.44) | copy-start | bytes 786436
  261.3 43.8 %copy-start.5 = (f32[128,512]{0,1:T(8,128)S(1)}, f32[128,512]{0,1:T(8,128)}, u32[]{:S(2)}) copy-start(f32[128,512]{0,1:T(8,128)} %copy.43) | copy-start | bytes 786436
  261.3 43.8 %copy-start.6 = (f32[128,512]{0,1:T(8,128)S(1)}, f32[128,512]{0,1:T(8,128)}, u32[]{:S(2)}) copy-start(f32[128,512]{0,1:T(8,128)} %copy.42) | copy-start | bytes 786436
Sparse Core Ops, SparseCore 0:
  10.6 34.4 all-gather.4
  47.3 61.3 all-gather.2
  129.4 37.4 reduce-scatter.4
  222.4 81.4 reduce-scatter.6
where the time goes:
time: 315 us; the launch traced here: 314 us
  waiting for transfers between devices  196 us (62%)
  blocking collectives  29.7 us (9%)
  matrix products  27.9 us (9%)
  local copies, waits for them, and re-layouts  27.4 us (9%)
  other arithmetic  15.7 us (5%)
  between operations  13.9 us (4%)
  starting transfers between devices  3.91 us (1%)
    all_gather x1, waiting for transfers between devices, sent_together(): lax.all_gather(both, axis, axis=dim, tiled=True)  63.5 us
    unnamed x5, waiting for transfers between devices  39.1 us
    reduce_scatter x1, waiting for transfers between devices, per_device(): lax.psum_scatter(gated_product.reshape(lax.axis_size('tp') * tok_rows, 2...  36.9 us
    all_gather x1, waiting for transfers between devices, per_device(): normed_rows = lax.all_gather(normed, 'tp', axis=1, tiled=True)  32.7 us
    all_to_all x1, blocking collectives, sent_to_all(): lax.all_to_all(jnp.broadcast_to(shard[None], (peers, *shard.shape)), axis...  29.7 us
    all_to_all x1, waiting for transfers between devices, summed_on_arrival(): lax.all_to_all(parts, axis, split_axis=0, concat_axis=0, tiled=True)  23.5 us
    unnamed x39, local copies, waits for them, and re-layouts  17.1 us
    dot_general x2, matrix products, contract_last(): lax.dot_general(first_op, second_op, (((1,), (1,)), ((), ())), preferred_...  7.09 us
  transfers between devices with their start and end apart: 5, of which 5 were waited for; matrix products, arithmetic and copies ran while one was open for 5% of the time, Pallas kernels for 0%

commit v1 on v0

--- a/solution.py
+++ b/solution.py
@@ -82,7 +82,12 @@
     input_rows = jnp.stack([late_input, early_input]).astype(jnp.float32)
     input_inverse = inverse_rms(input_rows)
     normed = (input_rows * input_inverse * pre_gain).astype(jnp.bfloat16)
-    normed_rows = lax.all_gather(normed, "tp", axis=1, tiled=True)
+    ring = [normed]
+    for hop in range(7):
+        ring.append(lax.ppermute(ring[-1], "tp", [(dev, (dev + 1) % 8) for dev in range(8)]))
+    normed_rows = jnp.roll(
+        jnp.concatenate(ring[::-1], axis=1), (lax.axis_index("tp") + 1) * ring[0].shape[1], axis=1
+    )
     gate_all, up_all, down_gradient_rows = sent_together(
         (gate_weight, up_weight, down_weight), "fs", 0, 1
     )

time: 315 us -> 302 us (0.959)
  blocking collectives: 29.7 us -> 0 us
  local copies, waits for them, and re-layouts: 27.4 us -> 39.3 us
  starting transfers between devices: 3.91 us -> 7.54 us
    ppermute x0 -> x7, waiting for transfers between devices: none -> 69.1 us  [per_device(): lax.ppermute(ring[-1], 'tp', [(dev, (dev + 1) % 8) for dev in range(8)])]
    all_gather x1, waiting for transfers between devices: 63.5 us -> 0.01 us  [sent_together(): lax.all_gather(both, axis, axis=dim, tiled=True)]
    all_gather x1 -> x0, waiting for transfers between devices: 32.7 us -> none  [per_device(): normed_rows = lax.all_gather(normed, 'tp', axis=1, tiled=True)]
    all_to_all x1 -> x0, blocking collectives: 29.7 us -> none  [sent_to_all(): lax.all_to_all(jnp.broadcast_to(shard[None], (peers, *shard.shape)), axis...]
    all_to_all x0 -> x1, waiting for transfers between devices: none -> 26.9 us  [sent_to_all(): lax.all_to_all(jnp.broadcast_to(shard[None], (peers, *shard.shape)), axis...]
    unnamed x39 -> x53, local copies, waits for them, and re-layouts: 17.1 us -> 25.4 us
    all_to_all x0 -> x1, starting transfers between devices: none -> 3.6 us  [sent_to_all(): lax.all_to_all(jnp.broadcast_to(shard[None], (peers, *shard.shape)), axis...]
    unnamed x5 -> x4, waiting for transfers between devices: 39.1 us -> 40.7 us
  transfers between devices with their start and end apart: 5 -> 12, of which waited for: 5 -> 11; matrix products, arithmetic and copies ran while one was open for 5% -> 8% of each run, Pallas kernels for 0% -> 0%
where the time goes in v1:
time: 302 us; the launch traced here: 301 us
  waiting for transfers between devices  197 us (65%)
  local copies, waits for them, and re-layouts  39.3 us (13%)
  matrix products  28.1 us (9%)
  other arithmetic  14.7 us (5%)
  between operations  14.1 us (5%)
  starting transfers between devices  7.54 us (2%)
    ppermute x7, waiting for transfers between devices, per_device(): lax.ppermute(ring[-1], 'tp', [(dev, (dev + 1) % 8) for dev in range(8)])  69.1 us
    unnamed x4, waiting for transfers between devices  40.7 us
    reduce_scatter x1, waiting for transfers between devices, per_device(): lax.psum_scatter(gated_product.reshape(lax.axis_size('tp') * tok_rows, 2...  38.1 us
    all_to_all x1, waiting for transfers between devices, sent_to_all(): lax.all_to_all(jnp.broadcast_to(shard[None], (peers, *shard.shape)), axis...  26.9 us
    unnamed x53, local copies, waits for them, and re-layouts  25.4 us
    all_to_all x1, waiting for transfers between devices, summed_on_arrival(): lax.all_to_all(parts, axis, split_axis=0, concat_axis=0, tiled=True)  22.6 us
    dot_general x2, matrix products, contract_last(): lax.dot_general(first_op, second_op, (((1,), (1,)), ((), ())), preferred_...  7.18 us
    convert_element_type x1, local copies, waits for them, and re-layouts, per_device(): gated_product.reshape(lax.axis_size('tp') * tok_rows, 2 * model_width)  6.4 us
  transfers between devices with their start and end apart: 12, of which 11 were waited for; matrix products, arithmetic and copies ran while one was open for 8% of the time, Pallas kernels for 0%

profile of v1, /device:TPU:0, one launch (start us, length us, event | category | flops | bytes accessed | tf_op | source)
XLA Modules:
  0.0 301.2 jit_solution(7106197401537910183)
XLA Ops:
  7.2 0.0 all-gather.2.cloned.1.call-start
  7.2 1.9 pad_maximum_fusion
  9.1 0.0 all-gather.2.cloned.1.call-update
  9.1 0.0 reduce-scatter.5.cloned.1.call-start
  9.2 1.2 multiply_reduce_fusion.1
  10.4 1.2 multiply_convert_fusion.2
  11.6 0.0 collective-permute-start
  11.7 9.8 %collective-permute-done = bf16[2,64,2048]{2,1,0:T(8,128)(2,1)S(1)} collective-permute-done((bf16[2,64,2048]{2,1,0:T(8,128)(2,1)S(1)}, bf16[2,64,2048]{2,1,0:T(8,128)(2,1)S(1)}, u32[]{:S(2)}, u32[]{:S(2)}) %collective-permute-start) | collective-permute-done | bytes 524320 | tf_op jit(solution)/shard_map/ppermute | solution.py:87
  21.5 9.8 %collective-permute-done.1 = bf16[2,64,2048]{2,1,0:T(8,128)(2,1)S(1)} collective-permute-done((bf16[2,64,2048]{2,1,0:T(8,128)(2,1)S(1)}, bf16[2,64,2048]{2,1,0:T(8,128)(2,1)S(1)}, u32[]{:S(2)}, u32[]{:S(2)}) %collective-permute-start.1) | collective-permute-done | bytes 524320 | tf_op jit(solution)/shard_map/ppermute | solution.py:87
  31.3 9.8 %collective-permute-done.2 = bf16[2,64,2048]{2,1,0:T(8,128)(2,1)S(1)} collective-permute-done((bf16[2,64,2048]{2,1,0:T(8,128)(2,1)S(1)}, bf16[2,64,2048]{2,1,0:T(8,128)(2,1)S(1)}, u32[]{:S(2)}, u32[]{:S(2)}) %collective-permute-start.2) | collective-permute-done | bytes 524320 | tf_op jit(solution)/shard_map/ppermute | solution.py:87
  41.1 9.8 %collective-permute-done.3 = bf16[2,64,2048]{2,1,0:T(8,128)(2,1)S(1)} collective-permute-done((bf16[2,64,2048]{2,1,0:T(8,128)(2,1)S(1)}, bf16[2,64,2048]{2,1,0:T(8,128)(2,1)S(1)}, u32[]{:S(2)}, u32[]{:S(2)}) %collective-permute-start.3) | collective-permute-done | bytes 524320 | tf_op jit(solution)/shard_map/ppermute | solution.py:87
  50.9 9.8 %collective-permute-done.4 = bf16[2,64,2048]{2,1,0:T(8,128)(2,1)S(1)} collective-permute-done((bf16[2,64,2048]{2,1,0:T(8,128)(2,1)S(1)}, bf16[2,64,2048]{2,1,0:T(8,128)(2,1)S(1)}, u32[]{:S(2)}, u32[]{:S(2)}) %collective-permute-start.4) | collective-permute-done | bytes 524320 | tf_op jit(solution)/shard_map/ppermute | solution.py:87
  60.7 9.9 %collective-permute-done.5 = bf16[2,64,2048]{2,1,0:T(8,128)(2,1)} collective-permute-done((bf16[2,64,2048]{2,1,0:T(8,128)(2,1)S(1)}, bf16[2,64,2048]{2,1,0:T(8,128)(2,1)}, u32[]{:S(2)}, u32[]{:S(2)}) %collective-permute-start.5) | collective-permute-done | bytes 524320 | tf_op jit(solution)/shard_map/ppermute | solution.py:87
  70.7 10.1 %collective-permute-done.6 = bf16[2,64,2048]{2,1,0:T(8,128)(2,1)} collective-permute-done((bf16[2,64,2048]{2,1,0:T(8,128)(2,1)}, bf16[2,64,2048]{2,1,0:T(8,128)(2,1)}, u32[]{:S(2)}, u32[]{:S(2)}) %collective-permute-start.6) | collective-permute-done | bytes 524320 | tf_op jit(solution)/shard_map/ppermute | solution.py:87
  80.8 1.1 constant_dynamic-update-slice_fusion.15
  81.9 1.1 constant_dynamic-update-slice_fusion.14
  83.2 0.2 constant_dynamic-update-slice_fusion.8
  83.4 1.1 constant_dynamic-update-slice_fusion.7
  84.5 1.1 constant_dynamic-update-slice_fusion.6
  85.8 0.2 constant_dynamic-update-slice_fusion
  86.0 3.2 %copy-done = bf16[2,1024,2048]{2,1,0:T(8,128)(2,1)} copy-done((bf16[2,1024,2048]{2,1,0:T(8,128)(2,1)}, bf16[2,1024,2048]{2,1,0:T(8,128)(2,1)S(1)}, u32[]{:S(2)}) %copy-start) | copy-done | bytes 8388632
  89.2 2.3 constant_dynamic-slice_fusion
  91.5 5.3 %fusion.7 = f32[1024,512]{1,0:T(8,128)S(1)} fusion(bf16[1024,2048]{1,0:T(8,128)(2,1)} %bitcast.78, bf16[2048,1536]{1,0:T(8,128)(2,1)} %all-gather.2.cloned.1.call-done), kind=kOutput, calls=%fused_computation.12 | convolution fusion | flops 2147483648 | bytes 8388608 | tf_op jit(solution)/shard_map/dot_general | solution.py:95
  96.8 0.6 copy-done.4
  97.5 3.9 %multiply_convert_fusion = (bf16[1024,512]{1,0:T(8,128)(2,1)S(1)}, f32[1024,512]{1,0:T(8,128)}) fusion(f32[1024,512]{1,0:T(8,128)S(1)} %fusion.7, bf16[1024,2048]{1,0:T(8,128)(2,1)S(1)} %bitcast.79, bf16[2048,1536]{1,0:T(8,128)(2,1)S(1)} %copy-done.4), kind=kOutput, calls=%fused_computation.6 | convolution fusion | flops 2150629376 | bytes 11534336 | tf_op jit(solution)/shard_map/dot_general | solution.py:96
  101.4 4.4 %convolution_convert_fusion = bf16[2048,2,512]{2,0,1:T(8,128)(2,1)} fusion(bf16[2,512,512]{2,1,0:T(8,128)(2,1)S(1)} %bitcast.81, bf16[2048,1536]{1,0:T(8,128)(2,1)S(1)} %copy-done.4), kind=kOutput, calls=%fused_computation.3 | convolution fusion | flops 2149580800 | bytes 7340032 | tf_op jit(solution)/shard_map/utx,ix->tui/dot_general | solution.py:100
  105.8 6.4 %copy.39 = bf16[512,4096]{1,0:T(8,128)(2,1)} copy(bf16[512,4096]{0,1:T(8,128)(2,1)} %bitcast.80) | data formatting | bytes 8388608 | tf_op jit(solution)/shard_map/convert_element_type | solution.py:104
  112.3 38.1 %reduce-scatter.5.cloned.1.call-done = bf16[64,4096]{1,0:T(8,128)(2,1)} async-done(((bf16[512,4096]{1,0:T(8,128)(2,1)}), bf16[64,4096]{1,0:T(8,128)(2,1)}) %reduce-scatter.5.cloned.1.call-update) | async-done | bytes 524304 | tf_op jit(solution)/shard_map/reduce_scatter | solution.py:103
  150.4 2.1 reshape.128
  152.4 1.6 fusion.33
  154.1 0.5 multiply_reduce_fusion
  154.6 0.1 copy.52
  154.6 0.3 fusion.21
  154.9 0.3 fusion.20
  155.2 1.6 broadcast_in_dim.2
  156.8 3.6 %all-to-all-start = ((bf16[8,64,2048]{2,1,0:T(8,128)(2,1)}), bf16[8,64,2048]{2,1,0:T(8,128)(2,1)S(1)}, u32[]{:S(2)}, u32[]{:S(2)}) async-start(bf16[8,64,2048]{2,1,0:T(8,128)(2,1)} %broadcast_in_dim.2), calls=%async_computation.1 | async-start | bytes 4194304 | tf_op jit(solution)/shard_map/all_to_all | solution.py:21
  160.4 0.2 reduce-scatter.7.cloned.1.call-start
  160.6 26.9 %all-to-all-done = bf16[8,64,2048]{2,1,0:T(8,128)(2,1)S(1)} async-done(((bf16[8,64,2048]{2,1,0:T(8,128)(2,1)}), bf16[8,64,2048]{2,1,0:T(8,128)(2,1)S(1)}, u32[]{:S(2)}, u32[]{:S(2)}) %all-to-all-start) | async-done | bytes 2097184 | tf_op jit(solution)/shard_map/all_to_all | solution.py:21
  187.5 1.3 fusion.24
  188.8 0.3 copy-done.11
  189.1 0.6 copy-done.12
  189.7 3.4 %multiply_convert_fusion.1 = (bf16[512,512]{1,0:T(8,128)(2,1)S(1)}, bf16[512,512]{1,0:T(8,128)(2,1)S(1)}) fusion(f32[1024,512]{1,0:T(8,128)S(1)} %copy-done.11, f32[1024,512]{1,0:T(8,128)S(1)} %copy-done.12, bf16[512,2048]{1,0:T(8,128)(2,1)S(1)} %bitcast.65, bf16[2048,1536]{1,0:T(8,128)(2,1)} %all-gather.2.cloned.1.call-done), kind=kOutput, calls=%fused_computation.23 | convolution fusion | flops 1077149696 | bytes 7340032 | tf_op jit(solution)/shard_map/dot_general | solution.py:127
  193.1 1.3 fusion.12
  194.4 1.3 fusion.13
  195.7 3.9 %fusion = bf16[2048,1536]{0,1:T(8,128)(2,1)} fusion(f32[2048,512]{0,1:T(8,128)S(1)} %fusion.24, f32[2048,512]{0,1:T(8,128)S(1)} %fusion.12, f32[2048,512]{0,1:T(8,128)S(1)} %fusion.13), kind=kLoop, calls=%fused_computation.1 | loop fusion | flops 12582912 | bytes 18874368 | tf_op jit(solution)/shard_map/convert_element_type | solution.py:162
  199.6 8.6 %copy.48 = bf16[2048,1536]{1,0:T(8,128)(2,1)} copy(bf16[2048,1536]{0,1:T(8,128)(2,1)} %fusion) | data formatting | bytes 12582912
  208.2 2.9 fusion.5
  211.1 4.3 %add_convert_fusion = bf16[512,2048]{1,0:T(8,128)(2,1)} fusion(f32[512,2048]{1,0:T(8,128)S(1)} %fusion.5, bf16[512,512]{1,0:T(8,128)(2,1)S(1)} %get-tuple-element.25, bf16[2048,1536]{1,0:T(8,128)(2,1)} %all-gather.2.cloned.1.call-done), kind=kOutput, calls=%fused_computation.2 | convolution fusion | flops 1075838976 | bytes 8912896 | tf_op jit(solution)/shard_map/dot_general | solution.py:50
  215.4 3.6 %all-to-all-start.1 = ((bf16[8,64,2048]{2,1,0:T(8,128)(2,1)}), bf16[8,64,2048]{2,1,0:T(8,128)(2,1)S(1)}, u32[]{:S(2)}, u32[]{:S(2)}) async-start(bf16[8,64,2048]{2,1,0:T(8,128)(2,1)} %bitcast.14), calls=%async_computation.2 | async-start | bytes 4194304 | tf_op jit(solution)/shard_map/all_to_all | solution.py:45
  219.1 0.8 copy.44
  219.9 0.8 copy.43
  220.7 1.8 copy.42
  222.5 1.0 maximum_convert_fusion
  223.6 22.6 %all-to-all-done.1 = bf16[8,64,2048]{2,1,0:T(8,128)(2,1)S(1)} async-done(((bf16[8,64,2048]{2,1,0:T(8,128)(2,1)}), bf16[8,64,2048]{2,1,0:T(8,128)(2,1)S(1)}, u32[]{:S(2)}, u32[]{:S(2)}) %all-to-all-start.1) | async-done | bytes 2097184 | tf_op jit(solution)/shard_map/all_to_all | solution.py:45
  246.1 0.4 reduce_sum.51
  246.5 0.2 multiply_reduce_fusion.2
  246.7 2.2 fusion.23
  248.9 40.7 %reduce-scatter.7.cloned.1.call-done = bf16[128,1536]{1,0:T(8,128)(2,1)} async-done(((bf16[2048,1536]{1,0:T(8,128)(2,1)}), bf16[128,1536]{1,0:T(8,128)(2,1)}) %reduce-scatter.7.cloned.1.call-update) | async-done | bytes 393232
  289.6 1.2 copy.49
  290.9 0.1 convert_element_type.69
  290.9 1.2 slice_add_fusion
  292.1 0.8 copy.45
  292.9 0.8 copy.46
  293.8 0.8 copy.47
  (54 shorter events, 0.5 us)
Async XLA Ops:
  7.2 76.0 %copy-start.1 = (bf16[64,2048]{1,0:T(8,128)(2,1)S(1)}, bf16[64,2048]{1,0:T(8,128)(2,1)}, u32[]{:S(2)}) copy-start(bf16[64,2048]{1,0:T(8,128)(2,1)} %param.12) | copy-start | bytes 786436
  7.2 76.0 %copy-start.2 = (bf16[64,2048]{1,0:T(8,128)(2,1)S(1)}, bf16[64,2048]{1,0:T(8,128)(2,1)}, u32[]{:S(2)}) copy-start(bf16[64,2048]{1,0:T(8,128)(2,1)} %param.11) | copy-start | bytes 786436
  7.2 76.0 %copy-start.8 = (f32[2048]{0:T(1024)S(1)}, f32[2048]{0:T(1024)}, u32[]{:S(2)}) copy-start(f32[2048]{0:T(1024)} %param.14) | copy-start | bytes 24580
  7.2 84.3 %all-gather.2.cloned.1.call-start = ((), (), s32[]{:S(2)}) async-start(), calls=%async_computation.4 | async-start | bytes 6684672 | tf_op jit(solution)/shard_map/all_gather | solution.py:16
  9.1 141.2 %reduce-scatter.5.cloned.1.call-start = ((), (), s32[]{:S(2)}) async-start(), calls=%async_computation.5 | async-start | bytes 4718592 | tf_op jit(solution)/shard_map/reduce_scatter | solution.py:103
  11.6 9.8 %collective-permute-start = (bf16[2,64,2048]{2,1,0:T(8,128)(2,1)S(1)}, bf16[2,64,2048]{2,1,0:T(8,128)(2,1)S(1)}, u32[]{:S(2)}, u32[]{:S(2)}) collective-permute-start(bf16[2,64,2048]{2,1,0:T(8,128)(2,1)S(1)} %multiply_convert_fusion.2), channel_id=1, source_target_pairs={{0,1},{1,2},{2,3},{3,4},{4,5},{5,6},{6,7},{7,0},{8,9},{9,10},{10,1... | collective-permute-start | bytes 1572872 | tf_op jit(solution)/shard_map/ppermute | solution.py:87
  21.5 9.8 %collective-permute-start.1 = (bf16[2,64,2048]{2,1,0:T(8,128)(2,1)S(1)}, bf16[2,64,2048]{2,1,0:T(8,128)(2,1)S(1)}, u32[]{:S(2)}, u32[]{:S(2)}) collective-permute-start(bf16[2,64,2048]{2,1,0:T(8,128)(2,1)S(1)} %collective-permute-done), channel_id=1, source_target_pairs={{0,1},{1,2},{2,3},{3,4},{4,5},{5,6},{6,7},{7,0},{8,9},{9,10},{10,1... | collective-permute-start | bytes 1572872 | tf_op jit(solution)/shard_map/ppermute | solution.py:87
  31.3 9.8 %collective-permute-start.2 = (bf16[2,64,2048]{2,1,0:T(8,128)(2,1)S(1)}, bf16[2,64,2048]{2,1,0:T(8,128)(2,1)S(1)}, u32[]{:S(2)}, u32[]{:S(2)}) collective-permute-start(bf16[2,64,2048]{2,1,0:T(8,128)(2,1)S(1)} %collective-permute-done.1), channel_id=1, source_target_pairs={{0,1},{1,2},{2,3},{3,4},{4,5},{5,6},{6,7},{7,0},{8,9},{9,10},{10,1... | collective-permute-start | bytes 1572872 | tf_op jit(solution)/shard_map/ppermute | solution.py:87
  41.1 9.8 %collective-permute-start.3 = (bf16[2,64,2048]{2,1,0:T(8,128)(2,1)S(1)}, bf16[2,64,2048]{2,1,0:T(8,128)(2,1)S(1)}, u32[]{:S(2)}, u32[]{:S(2)}) collective-permute-start(bf16[2,64,2048]{2,1,0:T(8,128)(2,1)S(1)} %collective-permute-done.2), channel_id=1, source_target_pairs={{0,1},{1,2},{2,3},{3,4},{4,5},{5,6},{6,7},{7,0},{8,9},{9,10},{10,1... | collective-permute-start | bytes 1572872 | tf_op jit(solution)/shard_map/ppermute | solution.py:87
  50.9 9.8 %collective-permute-start.4 = (bf16[2,64,2048]{2,1,0:T(8,128)(2,1)S(1)}, bf16[2,64,2048]{2,1,0:T(8,128)(2,1)S(1)}, u32[]{:S(2)}, u32[]{:S(2)}) collective-permute-start(bf16[2,64,2048]{2,1,0:T(8,128)(2,1)S(1)} %collective-permute-done.3), channel_id=1, source_target_pairs={{0,1},{1,2},{2,3},{3,4},{4,5},{5,6},{6,7},{7,0},{8,9},{9,10},{10,1... | collective-permute-start | bytes 1572872 | tf_op jit(solution)/shard_map/ppermute | solution.py:87
  60.7 9.9 %collective-permute-start.5 = (bf16[2,64,2048]{2,1,0:T(8,128)(2,1)S(1)}, bf16[2,64,2048]{2,1,0:T(8,128)(2,1)}, u32[]{:S(2)}, u32[]{:S(2)}) collective-permute-start(bf16[2,64,2048]{2,1,0:T(8,128)(2,1)S(1)} %collective-permute-done.4), channel_id=1, source_target_pairs={{0,1},{1,2},{2,3},{3,4},{4,5},{5,6},{6,7},{7,0},{8,9},{9,10},{10,1... | collective-permute-start | bytes 1572872 | tf_op jit(solution)/shard_map/ppermute | solution.py:87
  70.7 10.1 %collective-permute-start.6 = (bf16[2,64,2048]{2,1,0:T(8,128)(2,1)}, bf16[2,64,2048]{2,1,0:T(8,128)(2,1)}, u32[]{:S(2)}, u32[]{:S(2)}) collective-permute-start(bf16[2,64,2048]{2,1,0:T(8,128)(2,1)} %collective-permute-done.5), channel_id=1, source_target_pairs={{0,1},{1,2},{2,3},{3,4},{4,5},{5,6},{6,7},{7,0},{8,9},{9,10},{10,1... | collective-permute-start | bytes 1572872 | tf_op jit(solution)/shard_map/ppermute | solution.py:87
  86.0 3.3 %copy-start = (bf16[2,1024,2048]{2,1,0:T(8,128)(2,1)}, bf16[2,1024,2048]{2,1,0:T(8,128)(2,1)S(1)}, u32[]{:S(2)}) copy-start(bf16[2,1024,2048]{2,1,0:T(8,128)(2,1)S(1)} %constant_dynamic-update-slice_fusion) | copy-start | bytes 25165828
  91.5 5.3 %copy-start.3 = (bf16[2,512,2048]{2,1,0:T(8,128)(2,1)S(1)}, bf16[2,512,2048]{2,1,0:T(8,128)(2,1)}, u32[]{:S(2)}) copy-start(bf16[2,512,2048]{2,1,0:T(8,128)(2,1)} %constant_dynamic-slice_fusion) | copy-start | bytes 12582916
  91.5 5.9 %copy-start.4 = (bf16[2048,1536]{1,0:T(8,128)(2,1)S(1)}, bf16[2048,1536]{1,0:T(8,128)(2,1)}, u32[]{:S(2)}) copy-start(bf16[2048,1536]{1,0:T(8,128)(2,1)} %all-gather.2.cloned.1.call-done) | copy-start | bytes 18874372
  97.5 3.9 %copy-start.10 = (f32[1024,512]{1,0:T(8,128)}, f32[1024,512]{1,0:T(8,128)S(1)}, u32[]{:S(2)}) copy-start(f32[1024,512]{1,0:T(8,128)S(1)} %fusion.7) | copy-start | bytes 6291460
  105.8 6.4 %copy-start.9 = (f32[2048]{0:T(1024)S(1)}, f32[2048]{0:T(1024)}, u32[]{:S(2)}) copy-start(f32[2048]{0:T(1024)} %param.15) | copy-start | bytes 24580
  112.2 42.4 %copy-start.5 = (bf16[64,2048]{1,0:T(8,128)(2,1)S(1)}, bf16[64,2048]{1,0:T(8,128)(2,1)}, u32[]{:S(2)}) copy-start(bf16[64,2048]{1,0:T(8,128)(2,1)} %param.13) | copy-start | bytes 786436
  156.8 30.7 %all-to-all-start = ((bf16[8,64,2048]{2,1,0:T(8,128)(2,1)}), bf16[8,64,2048]{2,1,0:T(8,128)(2,1)S(1)}, u32[]{:S(2)}, u32[]{:S(2)}) async-start(bf16[8,64,2048]{2,1,0:T(8,128)(2,1)} %broadcast_in_dim.2), calls=%async_computation.1 | async-start | bytes 4194304 | tf_op jit(solution)/shard_map/all_to_all | solution.py:21
  160.4 129.2 %reduce-scatter.7.cloned.1.call-start = ((), (), s32[]{:S(2)}) async-start(), calls=%async_computation.6 | async-start | bytes 6684672
  187.5 1.6 copy-start.11
  187.5 2.2 copy-start.12
  187.5 5.6 %slice-start = ((s8[8388608]{0:T(1024)(128)(4,1)}), s8[4194304]{0:T(1024)(128)(4,1)S(1)}, s32[]{:S(2)}) async-start(s8[8388608]{0:T(1024)(128)(4,1)} %bitcast.66), calls=%async_computation.7 | async-start | bytes 8388608
  189.7 3.4 %slice-start.1 = ((s8[8388608]{0:T(1024)(128)(4,1)}), s8[4194304]{0:T(1024)(128)(4,1)S(1)}, s32[]{:S(2)}) async-start(s8[8388608]{0:T(1024)(128)(4,1)} %bitcast.66), calls=%async_computation.8 | async-start | bytes 8388608
  211.1 7.9 %copy-start.6 = (f32[128,512]{1,0:T(8,128)S(1)}, f32[128,512]{1,0:T(8,128)}, u32[]{:S(2)}) copy-start(f32[128,512]{1,0:T(8,128)} %param.21) | copy-start | bytes 786436
  211.1 8.8 %copy-start.7 = (f32[128,512]{1,0:T(8,128)S(1)}, f32[128,512]{1,0:T(8,128)}, u32[]{:S(2)}) copy-start(f32[128,512]{1,0:T(8,128)} %param.20) | copy-start | bytes 786436
  215.4 30.7 %all-to-all-start.1 = ((bf16[8,64,2048]{2,1,0:T(8,128)(2,1)}), bf16[8,64,2048]{2,1,0:T(8,128)(2,1)S(1)}, u32[]{:S(2)}, u32[]{:S(2)}) async-start(bf16[8,64,2048]{2,1,0:T(8,128)(2,1)} %bitcast.14), calls=%async_computation.2 | async-start | bytes 4194304 | tf_op jit(solution)/shard_map/all_to_all | solution.py:45
Sparse Core Ops, SparseCore 0:
  10.1 63.8 all-gather.1
  112.4 37.9 reduce-scatter.4
  208.3 81.2 reduce-scatter.6
